TPU v7x, 32 devices: a whole 2x2x4 slice. The times are simulated.
32 devices in a mesh: sp: 8 (over z, y), tp: 4 (over x, core).
Axes of the slice: x: 2, y: 2, z: 4, core: 2. Of those that a mesh axis runs over, the one named last changes fastest.
Arguments:
- prompt_input: bfloat16 [2304, 2048], P('sp'), may hold values from -6 to 6
- next_input: bfloat16 [2048], replicated, may hold values from -6 to 6
- norm_gain: float32 [2048], replicated, may hold values from 0.1 to 1.9
- w_key: bfloat16 [2048, 1024], P(None, 'tp'), may hold values from -0.125 to 0.125
- w_value: bfloat16 [2048, 1024], P(None, 'tp'), may hold values from -0.125 to 0.125
- w_query: bfloat16 [2048, 1024], P(None, 'tp'), may hold values from -0.125 to 0.125
- key_offset: float32 [2304, 8], P('sp', 'tp'), may hold values from -10 to 0, as said below
Outputs:
- key_cache: bfloat16 [8, 8, 36, 1024], P('sp', None, None, 'tp')
- value_cache: bfloat16 [8, 8, 36, 1024], P('sp', None, None, 'tp')
- reading: bfloat16 [1024], replicated
Inputs may be any that keep to these rules, and one draw needn't show every extreme that they name: `key_offset`: finite log-odds offsets, one per key and head.
All inputs are finite; a program needn't handle non-finite values.
Results may differ from a plain program's by a relative error of at most 0.011.
Values may be sent and summed in bfloat16 or wider, within the bound.
A program may use at most 64 MiB of HBM per device.

v0:
```python
import jax
import jax.numpy as jnp
from jax import lax
from jax.sharding import PartitionSpec as P

HEAD_DIM = 128


def norm_rows(row_block, gain_vec):
    wide_rows = row_block.astype(jnp.float32)
    inv_rms = lax.rsqrt(jnp.mean(wide_rows * wide_rows, axis=-1, keepdims=True) + 1e-06)
    return (wide_rows * inv_rms * gain_vec).astype(jnp.bfloat16)


def shards(prompt_input, next_input, norm_gain, w_key, w_value, w_query, key_offset):
    span_len = prompt_input.shape[0]
    head_width = w_key.shape[1]
    heads_here = head_width // HEAD_DIM
    score_scale = HEAD_DIM ** (-0.5)
    slots = lax.axis_size("sp")
    sub_len = span_len // slots
    normed = norm_rows(prompt_input, norm_gain)
    key_rows = jnp.dot(normed, w_key, preferred_element_type=jnp.float32).astype(jnp.bfloat16)
    value_rows = jnp.dot(normed, w_value, preferred_element_type=jnp.float32).astype(jnp.bfloat16)
    outgoing = jnp.stack([key_rows, value_rows]).reshape(2, slots, 1, sub_len, head_width)
    arrived = lax.all_to_all(outgoing, "sp", split_axis=1, concat_axis=2, tiled=True)
    key_cache = arrived[0]
    value_cache = arrived[1]
    new_query = jnp.dot(
        norm_rows(next_input[None, :], norm_gain), w_query, preferred_element_type=jnp.float32
    )
    new_query = new_query.astype(jnp.bfloat16).reshape(heads_here, HEAD_DIM)
    key_heads = key_rows.reshape(span_len, heads_here, HEAD_DIM)
    value_heads = value_rows.reshape(span_len, heads_here, HEAD_DIM)
    logits = (
        jnp.einsum("hd,shd->sh", new_query, key_heads, preferred_element_type=jnp.float32)
        * score_scale
        + key_offset
    )
    log_breaks = jax.nn.log_sigmoid(-logits)
    inner_sum = lax.cumsum(log_breaks, axis=0, reverse=True) - log_breaks
    block_totals = jnp.sum(log_breaks, axis=0)
    every_total = lax.all_gather(block_totals[None], "sp", axis=0, tiled=True)
    block_ids = lax.broadcasted_iota(jnp.int32, every_total.shape, 0)
    carried = jnp.sum(jnp.where(block_ids > lax.axis_index("sp"), every_total, 0.0), axis=0)
    weights = jnp.exp(jax.nn.log_sigmoid(logits) + inner_sum + carried[None, :])
    partial_value = jnp.einsum("sh,shd->hd", weights, value_heads.astype(jnp.float32))
    summed = lax.psum(partial_value, "sp")
    own_read = summed.reshape(head_width).astype(jnp.bfloat16)
    reading = lax.all_gather(own_read, "tp", axis=0, tiled=True)
    return (key_cache, value_cache, reading)


def solution(mesh):
    placed = (P("sp", None), P(), P(), P(None, "tp"), P(None, "tp"), P(None, "tp"), P("sp", "tp"))
    return jax.shard_map(
        shards,
        mesh=mesh,
        in_specs=placed,
        out_specs=(P("sp", None, None, "tp"), P("sp", None, None, "tp"), P()),
        check_vma=False,
    )
```

profile of v0, /device:TPU:0, one launch (start us, length us, event | category | flops | bytes accessed | tf_op | source)
XLA Modules:
  0.0 65.4 jit_solution(9334492287471043287)
XLA Ops:
  0.6 0.0 copy-start
  0.6 0.0 copy-start.1
  0.7 1.7 %fusion = f32[288]{0:T(512)S(1)} fusion(bf16[288,2048]{1,0:T(8,128)(2,1)} %param.7), kind=kLoop, calls=%fused_computation.2 | loop fusion | flops 1769184 | bytes 1180800 | tf_op jit(solution)/shard_map/reduce_sum | solution.py:11
  2.4 0.0 copy-done
  2.4 0.2 copy-done.1
  2.6 0.0 copy-start.5
  2.6 0.0 copy-start.6
  2.6 1.3 %convolution_convert_fusion = bf16[288,256]{1,0:T(8,128)(2,1)S(1)} fusion(bf16[2048,256]{1,0:T(8,128)(2,1)S(1)} %copy-done, bf16[288,2048]{1,0:T(8,128)(2,1)S(1)} %copy-done.1, f32[2048]{0:T(1024)} %param.9, f32[288]{0:T(512)S(1)} %add_rsqrt_fusion), kind=kOutput, calls=%fused_computation.5 | convolution fusion | flops 304422912 | bytes 2385024 | tf_op jit(solution)/shard_map/dot_general | solution.py:24
  3.9 0.0 copy-done.5
  3.9 0.0 copy-done.6
  3.9 0.5 convolution_convert_fusion.1
  4.5 0.0 copy-start.3
  4.5 0.0 copy-start.2
  4.6 0.0 copy-start.7
  4.6 0.0 copy-start.4
  4.6 1.0 %copy.17 = bf16[2,8,1,36,256]{4,0,3,2,1:T(2,128)(2,1)} copy(bf16[2,8,1,36,256]{4,3,1,2,0:T(8,128)(2,1)S(1)} %pad_maximum_fusion) | data formatting | bytes 589824 | tf_op jit(solution)/shard_map/stack | solution.py:25
  5.6 7.3 %all-to-all-start = ((bf16[2,8,1,36,256]{4,0,3,2,1:T(2,128)(2,1)}), bf16[2,8,1,36,256]{4,0,3,2,1:T(2,128)(2,1)S(1)}, u32[]{:S(2)}, u32[]{:S(2)}) async-start(bf16[2,8,1,36,256]{4,0,3,2,1:T(2,128)(2,1)} %copy.17), calls=%async_computation | async-start | bytes 589824 | tf_op jit(solution)/shard_map/all_to_all | solution.py:26
  13.0 0.0 copy-done.3
  13.0 0.6 fusion.11
  14.3 0.0 copy-done.2
  14.3 0.2 fusion.21
  14.5 0.1 fusion.8
  14.7 0.0 copy-done.7
  14.7 0.6 dynamic-slice
  16.0 0.0 copy-done.4
  16.0 0.1 fusion.19
  16.1 0.1 negate_dynamic-update-slice_fusion
  16.2 21.8 %all-reduce.1 = f32[16]{0:T(128)S(1)} all-reduce(f32[16]{0:T(128)S(1)} %negate_dynamic-update-slice_fusion), channel_id=2, replica_groups=mesh['sp'=8,'tp'=4] {'sp'}, use_global_device_ids=true, to_apply=%add.1 | all-reduce | flops 16 | bytes 128
  38.1 2.5 %reduce-window.6 = f32[2,3,128]{2,1,0:T(4,128)S(1)} reduce-window(f32[2,3,128]{2,1,0:T(4,128)S(1)} %reshape.81, f32[]{:T(128)} %constant.20.clone.1), window={size=1x1x128 pad=0_0x0_0x0_127}, to_apply=%region_2.3 | reduce-window | flops 97536 | bytes 6148 | tf_op jit(solution)/shard_map/reduce-window
  40.6 0.1 slice_reduce_fusion
  40.7 0.2 reduce-window.9
  40.9 0.1 slice.21
  40.9 0.1 add_bitcast_fusion
  41.0 0.1 reshape.84
  41.1 0.1 select_reduce_fusion
  41.2 0.1 exponential_bitcast_fusion
  41.3 0.1 fusion.5
  41.4 17.1 %psum.7 = bf16[2,128]{1,0:T(2,128)(2,1)S(1)} all-reduce(f32[2,128]{1,0:T(2,128)S(1)} %bitcast.64), channel_id=1, replica_groups=mesh['sp'=8,'tp'=4] {'sp'}, use_global_device_ids=true, to_apply=%region_6.7 | all-reduce | flops 256 | bytes 1536 | tf_op jit(solution)/shard_map/psum | solution.py:48
  58.6 5.1 %all-gather.1 = bf16[4,1,256]{2,1,0:T(2,128)(2,1)S(1)} all-gather(bf16[1,1,256]{2,1,0:T(2,128)(2,1)S(1)} %reshape.88), channel_id=1, replica_groups=mesh['sp'=8,'tp'=4] {'tp'}, dimensions={0}, use_global_device_ids=true | all-gather | bytes 2560 | tf_op jit(solution)/shard_map/all_gather | solution.py:50
  63.6 0.6 copy.31
  64.2 0.0 all-to-all-done
  64.2 0.4 fusion.20
  64.6 0.8 %copy_bitcast_fusion = (bf16[1,8,36,256]{3,1,2,0:T(8,128)(2,1)}, bf16[1,8,36,256]{3,1,2,0:T(8,128)(2,1)}) fusion(bf16[1,8,1,36,256]{4,0,3,2,1:T(2,128)(2,1)S(1)} %get-tuple-element.11, bf16[1,8,1,36,256]{4,0,3,2,1:T(2,128)(2,1)S(1)} %get-tuple-element.12), kind=kLoop, calls=%fused_computation.14 | loop fusion | bytes 589824 | tf_op jit(solution)/shard_map/squeeze | solution.py:28
  (15 shorter events, 0.2 us)
Async XLA Ops:
  0.6 1.8 %copy-start = (bf16[2048,256]{1,0:T(8,128)(2,1)S(1)}, bf16[2048,256]{1,0:T(8,128)(2,1)}, u32[]{:S(2)}) copy-start(bf16[2048,256]{1,0:T(8,128)(2,1)} %param.11) | copy-start | bytes 3145732
  0.6 1.9 %copy-start.1 = (bf16[288,2048]{1,0:T(8,128)(2,1)S(1)}, bf16[288,2048]{1,0:T(8,128)(2,1)}, u32[]{:S(2)}) copy-start(bf16[288,2048]{1,0:T(8,128)(2,1)} %param.7) | copy-start | bytes 3538948
  2.6 1.3 %copy-start.5 = (f32[2048]{0:T(1024)S(1)}, f32[2048]{0:T(1024)}, u32[]{:S(2)}) copy-start(f32[2048]{0:T(1024)} %param.9) | copy-start | bytes 24580
  2.6 1.3 %copy-start.6 = (bf16[2048,256]{1,0:T(8,128)(2,1)S(1)}, bf16[2048,256]{1,0:T(8,128)(2,1)}, u32[]{:S(2)}) copy-start(bf16[2048,256]{1,0:T(8,128)(2,1)} %param.10) | copy-start | bytes 3145732
  4.5 8.5 %copy-start.3 = (bf16[2048]{0:T(1024)(128)(2,1)S(1)}, bf16[2048]{0:T(1024)(128)(2,1)}, u32[]{:S(2)}) copy-start(bf16[2048]{0:T(1024)(128)(2,1)} %param.8) | copy-start | bytes 12292
  4.5 9.8 %copy-start.2 = (bf16[2048,256]{1,0:T(8,128)(2,1)S(1)}, bf16[2048,256]{1,0:T(8,128)(2,1)}, u32[]{:S(2)}) copy-start(bf16[2048,256]{1,0:T(8,128)(2,1)} %param.12) | copy-start | bytes 3145732
  4.6 10.1 %copy-start.7 = (u32[32]{0:T(128)S(1)}, u32[32]{0:T(128)}, u32[]{:S(2)}) copy-start(u32[32]{0:T(128)} %constant.31) | copy-start | bytes 388
  4.6 11.3 %copy-start.4 = (f32[288,2]{0,1:T(2,128)S(1)}, f32[288,2]{0,1:T(2,128)}, u32[]{:S(2)}) copy-start(f32[288,2]{0,1:T(2,128)} %param.13) | copy-start | bytes 6916
  5.6 58.6 %all-to-all-start = ((bf16[2,8,1,36,256]{4,0,3,2,1:T(2,128)(2,1)}), bf16[2,8,1,36,256]{4,0,3,2,1:T(2,128)(2,1)S(1)}, u32[]{:S(2)}, u32[]{:S(2)}) async-start(bf16[2,8,1,36,256]{4,0,3,2,1:T(2,128)(2,1)} %copy.17), calls=%async_computation | async-start | bytes 589824 | tf_op jit(solution)/shard_map/all_to_all | solution.py:26
where the time goes:
time: 65.7 us; the launch traced here: 65.4 us
  blocking collectives  44 us (67%)
  starting transfers between devices  7.31 us (11%)
  other arithmetic  5.61 us (9%)
  local copies, waits for them, and re-layouts  3.98 us (6%)
  matrix products  2.36 us (4%)
  between operations  2.15 us (3%)
    unnamed x1, blocking collectives  21.8 us
    psum x1, blocking collectives, shards(): summed = lax.psum(partial_value, 'sp')  17.1 us
    all_to_all x1, starting transfers between devices, shards(): lax.all_to_all(outgoing, 'sp', split_axis=1, concat_axis=2, tiled=True)  7.31 us
    all_gather x1, blocking collectives, shards(): reading = lax.all_gather(own_read, 'tp', axis=0, tiled=True)  5.05 us
    another operation x2, other arithmetic  2.71 us
    reduce_sum x2, other arithmetic, norm_rows(): jnp.mean(wide_rows * wide_rows, axis=-1, keepdims=True) + 1e-06  2.34 us
    unnamed x21, local copies, waits for them, and re-layouts  1.43 us
  transfers between devices with their start and end apart: 1, of which 0 were waited for; matrix products, arithmetic and copies ran while one was open for 9% of the time, Pallas kernels for 0%

commit v1 on v0

--- a/solution.py
+++ b/solution.py
@@ -47,7 +47,12 @@
     partial_value = jnp.einsum("sh,shd->hd", weights, value_heads.astype(jnp.float32))
     summed = lax.psum(partial_value, "sp")
     own_read = summed.reshape(head_width).astype(jnp.bfloat16)
-    reading = lax.all_gather(own_read, "tp", axis=0, tiled=True)
+    ring = [own_read]
+    for hop in range(3):
+        ring.append(lax.ppermute(ring[-1], "tp", [(dev, (dev + 1) % 4) for dev in range(4)]))
+    reading = jnp.roll(
+        jnp.concatenate(ring[::-1], axis=0), (lax.axis_index("tp") + 1) * ring[0].shape[0], axis=0
+    )
     return (key_cache, value_cache, reading)
 
 

time: 65.7 us -> 71.3 us (1.085)
  waiting for transfers between devices: 0.01 us -> 8.96 us
  blocking collectives: 44 us -> 39 us
  local copies, waits for them, and re-layouts: 3.98 us -> 5.61 us
    ppermute x0 -> x3, waiting for transfers between devices: none -> 8.96 us  [shards(): lax.ppermute(ring[-1], 'tp', [(dev, (dev + 1) % 4) for dev in range(4)])]
    all_gather x1 -> x0, blocking collectives: 5.05 us -> none  [shards(): reading = lax.all_gather(own_read, 'tp', axis=0, tiled=True)]
    unnamed x21 -> x26, local copies, waits for them, and re-layouts: 1.43 us -> 2.2 us
  transfers between devices with their start and end apart: 1 -> 4, of which waited for: 0 -> 3; matrix products, arithmetic and copies ran while one was open for 9% -> 10% of each run, Pallas kernels for 0% -> 0%
where the time goes in v1:
time: 71.3 us; the launch traced here: 71 us
  blocking collectives  39 us (55%)
  waiting for transfers between devices  8.96 us (13%)
  starting transfers between devices  7.35 us (10%)
  local copies, waits for them, and re-layouts  5.61 us (8%)
  other arithmetic  5.59 us (8%)
  matrix products  2.36 us (3%)
  between operations  2.17 us (3%)
    unnamed x1, blocking collectives  21.8 us
    psum x1, blocking collectives, shards(): summed = lax.psum(partial_value, 'sp')  17.1 us
    ppermute x3, waiting for transfers between devices, shards(): lax.ppermute(ring[-1], 'tp', [(dev, (dev + 1) % 4) for dev in range(4)])  8.96 us
    all_to_all x1, starting transfers between devices, shards(): lax.all_to_all(outgoing, 'sp', split_axis=1, concat_axis=2, tiled=True)  7.31 us
    another operation x2, other arithmetic  2.71 us
    reduce_sum x2, other arithmetic, norm_rows(): jnp.mean(wide_rows * wide_rows, axis=-1, keepdims=True) + 1e-06  2.34 us
    unnamed x26, local copies, waits for them, and re-layouts  2.2 us
  transfers between devices with their start and end apart: 4, of which 3 were waited for; matrix products, arithmetic and copies ran while one was open for 10% of the time, Pallas kernels for 0%

profile of v1, /device:TPU:0, one launch (start us, length us, event | category | flops | bytes accessed | tf_op | source)
XLA Modules:
  0.0 71.0 jit_solution(10630098266762559142)
XLA Ops:
  0.6 0.0 copy-start
  0.6 0.0 copy-start.1
  0.7 1.7 %fusion = f32[288]{0:T(512)S(1)} fusion(bf16[288,2048]{1,0:T(8,128)(2,1)} %param.7), kind=kLoop, calls=%fused_computation.2 | loop fusion | flops 1769184 | bytes 1180800 | tf_op jit(solution)/shard_map/reduce_sum | solution.py:11
  2.4 0.0 copy-done
  2.4 0.2 copy-done.1
  2.6 0.0 copy-start.5
  2.6 0.0 copy-start.6
  2.6 1.3 %convolution_convert_fusion = bf16[288,256]{1,0:T(8,128)(2,1)S(1)} fusion(bf16[2048,256]{1,0:T(8,128)(2,1)S(1)} %copy-done, bf16[288,2048]{1,0:T(8,128)(2,1)S(1)} %copy-done.1, f32[2048]{0:T(1024)} %param.9, f32[288]{0:T(512)S(1)} %add_rsqrt_fusion), kind=kOutput, calls=%fused_computation.5 | convolution fusion | flops 304422912 | bytes 2385024 | tf_op jit(solution)/shard_map/dot_general | solution.py:24
  3.9 0.0 copy-done.5
  3.9 0.0 copy-done.6
  3.9 0.5 convolution_convert_fusion.1
  4.5 0.0 copy-start.3
  4.5 0.0 copy-start.2
  4.6 0.0 copy-start.7
  4.6 0.0 copy-start.4
  4.6 1.0 %copy.17 = bf16[2,8,1,36,256]{4,0,3,2,1:T(2,128)(2,1)} copy(bf16[2,8,1,36,256]{4,3,1,2,0:T(8,128)(2,1)S(1)} %pad_maximum_fusion) | data formatting | bytes 589824 | tf_op jit(solution)/shard_map/stack | solution.py:25
  5.6 7.3 %all-to-all-start = ((bf16[2,8,1,36,256]{4,0,3,2,1:T(2,128)(2,1)}), bf16[2,8,1,36,256]{4,0,3,2,1:T(2,128)(2,1)S(1)}, u32[]{:S(2)}, u32[]{:S(2)}) async-start(bf16[2,8,1,36,256]{4,0,3,2,1:T(2,128)(2,1)} %copy.17), calls=%async_computation | async-start | bytes 589824 | tf_op jit(solution)/shard_map/all_to_all | solution.py:26
  13.0 0.0 copy-done.3
  13.0 0.6 fusion.11
  14.3 0.0 copy-done.2
  14.3 0.2 fusion.21
  14.5 0.1 fusion.8
  14.7 0.0 copy-done.7
  14.7 0.6 dynamic-slice
  16.0 0.0 copy-done.4
  16.0 0.1 fusion.19
  16.1 0.1 negate_dynamic-update-slice_fusion
  16.2 21.8 %all-reduce.1 = f32[16]{0:T(128)S(1)} all-reduce(f32[16]{0:T(128)S(1)} %negate_dynamic-update-slice_fusion), channel_id=2, replica_groups=mesh['sp'=8,'tp'=4] {'sp'}, use_global_device_ids=true, to_apply=%add.1 | all-reduce | flops 16 | bytes 128
  38.1 2.5 %reduce-window.6 = f32[2,3,128]{2,1,0:T(4,128)S(1)} reduce-window(f32[2,3,128]{2,1,0:T(4,128)S(1)} %reshape.81, f32[]{:T(128)} %constant.42.clone.1), window={size=1x1x128 pad=0_0x0_0x0_127}, to_apply=%region_2.3 | reduce-window | flops 97536 | bytes 6148 | tf_op jit(solution)/shard_map/reduce-window
  40.6 0.1 slice_reduce_fusion
  40.7 0.2 reduce-window.9
  40.9 0.1 slice.21
  40.9 0.1 add_bitcast_fusion
  41.0 0.1 reshape.84
  41.1 0.1 select_reduce_fusion
  41.2 0.1 exponential_bitcast_fusion
  41.3 0.1 fusion.5
  41.4 17.1 %psum.7 = bf16[2,128]{1,0:T(2,128)(2,1)S(1)} all-reduce(f32[2,128]{1,0:T(2,128)S(1)} %bitcast.66), channel_id=1, replica_groups=mesh['sp'=8,'tp'=4] {'sp'}, use_global_device_ids=true, to_apply=%region_6.7 | all-reduce | flops 256 | bytes 1536 | tf_op jit(solution)/shard_map/psum | solution.py:48
  58.5 0.0 collective-permute-start
  58.6 3.0 %collective-permute-done = bf16[256]{0:T(256)(128)(2,1)S(1)} collective-permute-done((bf16[256]{0:T(256)(128)(2,1)S(1)}, bf16[256]{0:T(256)(128)(2,1)S(1)}, u32[]{:S(2)}, u32[]{:S(2)}) %collective-permute-start) | collective-permute-done | bytes 544 | tf_op jit(solution)/shard_map/ppermute | solution.py:52
  61.6 0.0 collective-permute-start.1
  61.6 3.0 %collective-permute-done.1 = bf16[256]{0:T(256)(128)(2,1)S(1)} collective-permute-done((bf16[256]{0:T(256)(128)(2,1)S(1)}, bf16[256]{0:T(256)(128)(2,1)S(1)}, u32[]{:S(2)}, u32[]{:S(2)}) %collective-permute-start.1) | collective-permute-done | bytes 544 | tf_op jit(solution)/shard_map/ppermute | solution.py:52
  64.6 0.0 collective-permute-start.2
  64.6 3.0 %collective-permute-done.2 = bf16[256]{0:T(256)(128)(2,1)S(1)} collective-permute-done((bf16[256]{0:T(256)(128)(2,1)S(1)}, bf16[256]{0:T(256)(128)(2,1)S(1)}, u32[]{:S(2)}, u32[]{:S(2)}) %collective-permute-start.2) | collective-permute-done | bytes 544 | tf_op jit(solution)/shard_map/ppermute | solution.py:52
  67.6 0.2 dynamic-update-slice.1
  67.7 0.2 dynamic-update-slice.2
  67.9 0.2 dynamic-update-slice.3
  68.1 0.2 dynamic-update-slice.4
  68.4 0.2 dynamic-update-slice.5
  68.5 0.2 dynamic-update-slice.6
  68.7 0.2 dynamic-update-slice.7
  68.9 0.2 dynamic-update-slice.8
  69.1 0.7 dynamic_slice.4
  69.8 0.0 all-to-all-done
  69.8 0.4 fusion.20
  70.2 0.8 %copy_bitcast_fusion = (bf16[1,8,36,256]{3,1,2,0:T(8,128)(2,1)}, bf16[1,8,36,256]{3,1,2,0:T(8,128)(2,1)}) fusion(bf16[1,8,1,36,256]{4,0,3,2,1:T(2,128)(2,1)S(1)} %get-tuple-element.11, bf16[1,8,1,36,256]{4,0,3,2,1:T(2,128)(2,1)S(1)} %get-tuple-element.12), kind=kLoop, calls=%fused_computation.14 | loop fusion | bytes 589824 | tf_op jit(solution)/shard_map/squeeze | solution.py:28
  (14 shorter events, 0.2 us)
Async XLA Ops:
  0.6 1.8 %copy-start = (bf16[2048,256]{1,0:T(8,128)(2,1)S(1)}, bf16[2048,256]{1,0:T(8,128)(2,1)}, u32[]{:S(2)}) copy-start(bf16[2048,256]{1,0:T(8,128)(2,1)} %param.11) | copy-start | bytes 3145732
  0.6 1.9 %copy-start.1 = (bf16[288,2048]{1,0:T(8,128)(2,1)S(1)}, bf16[288,2048]{1,0:T(8,128)(2,1)}, u32[]{:S(2)}) copy-start(bf16[288,2048]{1,0:T(8,128)(2,1)} %param.7) | copy-start | bytes 3538948
  2.6 1.3 %copy-start.5 = (f32[2048]{0:T(1024)S(1)}, f32[2048]{0:T(1024)}, u32[]{:S(2)}) copy-start(f32[2048]{0:T(1024)} %param.9) | copy-start | bytes 24580
  2.6 1.3 %copy-start.6 = (bf16[2048,256]{1,0:T(8,128)(2,1)S(1)}, bf16[2048,256]{1,0:T(8,128)(2,1)}, u32[]{:S(2)}) copy-start(bf16[2048,256]{1,0:T(8,128)(2,1)} %param.10) | copy-start | bytes 3145732
  4.5 8.5 %copy-start.3 = (bf16[2048]{0:T(1024)(128)(2,1)S(1)}, bf16[2048]{0:T(1024)(128)(2,1)}, u32[]{:S(2)}) copy-start(bf16[2048]{0:T(1024)(128)(2,1)} %param.8) | copy-start | bytes 12292
  4.5 9.8 %copy-start.2 = (bf16[2048,256]{1,0:T(8,128)(2,1)S(1)}, bf16[2048,256]{1,0:T(8,128)(2,1)}, u32[]{:S(2)}) copy-start(bf16[2048,256]{1,0:T(8,128)(2,1)} %param.12) | copy-start | bytes 3145732
  4.6 10.1 %copy-start.7 = (u32[32]{0:T(128)S(1)}, u32[32]{0:T(128)}, u32[]{:S(2)}) copy-start(u32[32]{0:T(128)} %constant.60) | copy-start | bytes 388
  4.6 11.3 %copy-start.4 = (f32[288,2]{0,1:T(2,128)S(1)}, f32[288,2]{0,1:T(2,128)}, u32[]{:S(2)}) copy-start(f32[288,2]{0,1:T(2,128)} %param.13) | copy-start | bytes 6916
  5.6 64.1 %all-to-all-start = ((bf16[2,8,1,36,256]{4,0,3,2,1:T(2,128)(2,1)}), bf16[2,8,1,36,256]{4,0,3,2,1:T(2,128)(2,1)S(1)}, u32[]{:S(2)}, u32[]{:S(2)}) async-start(bf16[2,8,1,36,256]{4,0,3,2,1:T(2,128)(2,1)} %copy.17), calls=%async_computation | async-start | bytes 589824 | tf_op jit(solution)/shard_map/all_to_all | solution.py:26
  58.5 3.0 %collective-permute-start = (bf16[256]{0:T(256)(128)(2,1)S(1)}, bf16[256]{0:T(256)(128)(2,1)S(1)}, u32[]{:S(2)}, u32[]{:S(2)}) collective-permute-start(bf16[256]{0:T(256)(128)(2,1)S(1)} %bitcast.62), channel_id=1, source_target_pairs={{0,1},{1,2},{2,3},{3,0},{4,5},{5,6},{6,7},{7,4},{8,9},{9,10},{10,1... | collective-permute-start | bytes 1544 | tf_op jit(solution)/shard_map/ppermute | solution.py:52
  61.6 3.0 %collective-permute-start.1 = (bf16[256]{0:T(256)(128)(2,1)S(1)}, bf16[256]{0:T(256)(128)(2,1)S(1)}, u32[]{:S(2)}, u32[]{:S(2)}) collective-permute-start(bf16[256]{0:T(256)(128)(2,1)S(1)} %collective-permute-done), channel_id=1, source_target_pairs={{0,1},{1,2},{2,3},{3,0},{4,5},{5,6},{6,7},{7,4},{8,9},{9,10},{10,1... | collective-permute-start | bytes 1544 | tf_op jit(solution)/shard_map/ppermute | solution.py:52
  64.6 3.0 %collective-permute-start.2 = (bf16[256]{0:T(256)(128)(2,1)S(1)}, bf16[256]{0:T(256)(128)(2,1)S(1)}, u32[]{:S(2)}, u32[]{:S(2)}) collective-permute-start(bf16[256]{0:T(256)(128)(2,1)S(1)} %collective-permute-done.1), channel_id=1, source_target_pairs={{0,1},{1,2},{2,3},{3,0},{4,5},{5,6},{6,7},{7,4},{8,9},{9,10},{10,1... | collective-permute-start | bytes 1544 | tf_op jit(solution)/shard_map/ppermute | solution.py:52
